TPU v7x, 32 devices: a whole 2x2x4 slice. The times are simulated.
32 devices in a mesh: sp: 4 (over z), tp: 8 (over y, x, core).
Axes of the slice: x: 2, y: 2, z: 4, core: 2. Of those that a mesh axis runs over, the one named last changes fastest.
Arguments:
- latent: bfloat16 [1024, 4096], P(('sp', 'tp')), may hold values from -16 to 16
- context: bfloat16 [256, 4096], P('sp'), may hold values from -16 to 16
- cond: bfloat16 [4096], P('sp'), may hold values from -6 to 6
- cond_ctx: bfloat16 [4096], P('sp'), may hold values from -6 to 6
- mod_shift_w: bfloat16 [4096, 4096], P('sp', 'tp'), may hold values from -0.15625 to 0.15625
- mod_scale_w: bfloat16 [4096, 4096], P('sp', 'tp'), may hold values from -0.15625 to 0.15625
- mod_gate_w: bfloat16 [4096, 4096], P('sp', 'tp'), may hold values from -0.15625 to 0.15625
- norm_gain: bfloat16 [4096], replicated, may hold values from 0.099609375 to 1.8984375
- proj_z: bfloat16 [4096, 4096], P(None, 'tp'), may hold values from -0.09375 to 0.09375
- proj_x: bfloat16 [4096, 4096], P(None, 'tp'), may hold values from -0.09375 to 0.09375
- proj_b: bfloat16 [4096, 8192], P(None, 'tp'), may hold values from -0.09375 to 0.09375
- proj_c: bfloat16 [4096, 8192], P(None, 'tp'), may hold values from -0.09375 to 0.09375
- proj_dt: bfloat16 [4096, 128], replicated, may hold values from -0.09375 to 0.09375
- conv_x: bfloat16 [3, 4096], P(None, 'tp'), may hold values from -3.5 to 3.5
- conv_b: bfloat16 [3, 8192], P(None, 'tp'), may hold values from -3.5 to 3.5
- conv_c: bfloat16 [3, 8192], P(None, 'tp'), may hold values from -3.5 to 3.5
- dt_bias: float32 [128], P('tp'), may hold values from -1 to 1
- decay_log: float32 [128], P('tp'), may hold values from -11.6 to -2.9
- head_gain: bfloat16 [4096], P('tp'), may hold values from 0.099609375 to 1.8984375
- proj_out: bfloat16 [4096, 4096], P(None, 'tp'), may hold values from -0.09375 to 0.09375
Outputs:
- mixed: bfloat16 [1024, 4096], P(('sp', 'tp'))
All inputs are finite; a program needn't handle non-finite values.
Results may differ from a plain program's by a relative error of at most 0.0065.
Values may be sent and summed in bfloat16 or wider, within the bound.
A program may use at most 128 MiB of HBM per device.

v0:
```python
import functools

import jax
import jax.numpy as jnp
from jax import lax
from jax.experimental import pallas as pl
from jax.experimental.pallas import tpu as pltpu
from jax.sharding import PartitionSpec as P

HEAD_DIM = 64
BLOCK = 128


EPS = 1e-06


def extended(array, sides, width):
    for axis, dim in sides:
        count, length = (lax.axis_size(axis), array.shape[dim])
        up = [(i, (i + 1) % count) for i in range(count - 1)]
        down = [(j, i) for i, j in up]
        last = lax.slice_in_dim(array, length - width, length, axis=dim)
        first = lax.slice_in_dim(array, 0, width, axis=dim)
        before = lax.ppermute(last, axis, up)
        after = lax.ppermute(first, axis, down)
        array = jnp.concatenate([before, array, after], axis=dim)
    return array


def entering_2(array, axis, combine, identity, reverse):
    count, place = (lax.axis_size(axis), lax.axis_index(axis))
    everything = jax.tree.map(
        lambda part, kind: lax.all_gather(part.astype(kind), axis),
        array,
        (jnp.bfloat16, jnp.bfloat16),
    )
    start = jax.tree.map(
        lambda part, zero: jnp.broadcast_to(jnp.asarray(zero, part.dtype), part.shape),
        array,
        identity,
    )

    def hop(k, before):
        at = count - 1 - k if reverse else k
        reached = at > place if reverse else at < place
        new = combine(
            before, jax.tree.map(lambda part, own: part[at].astype(own.dtype), everything, array)
        )
        return jax.tree.map(lambda a, b: jnp.where(reached, a, b), new, before)

    return lax.fori_loop(0, count, hop, start)


def modulated_norm(rows, gain, shift, scale):
    wide = rows.astype(jnp.float32)
    normed = (
        wide
        * lax.rsqrt(jnp.mean(wide * wide, axis=-1, keepdims=True) + EPS)
        * gain.astype(jnp.float32)
    )
    return (normed * (1.0 + scale) + shift).astype(jnp.bfloat16)


def project(rows, weights):
    outputs = [
        jnp.dot(rows, w, preferred_element_type=jnp.float32).astype(jnp.bfloat16) for w in weights
    ]
    return lax.optimization_barrier(outputs)


def centred_conv(padded, taps):
    wide = padded.astype(jnp.float32)
    weights = taps.astype(jnp.float32)
    length = padded.shape[0] - 2
    return jax.nn.silu(
        weights[0] * wide[:length] + weights[1] * wide[1 : length + 1] + weights[2] * wide[2:]
    )


def zero_pad(values):
    return jnp.pad(values, ((1, 1), (0, 0)))


def block_states(values, writes, step_size, decay_rate, block):
    length, heads, width = values.shape
    state = writes.shape[2]
    count = length // block
    log_decay = jnp.cumsum(-(step_size * decay_rate).reshape(count, block, heads), axis=1)
    scaled_values = (values * step_size[:, :, None]).reshape(count, block, heads, width)
    write_blocks = writes.reshape(count, block, heads, state)
    tail = jnp.exp(log_decay[:, -1:] - log_decay)
    block_sums = jnp.einsum(
        "kshn,ksh,kshp->khpn", write_blocks, tail, scaled_values, precision=lax.Precision.HIGHEST
    )
    block_decay = jnp.exp(log_decay[:, -1])

    def advance(carry, inputs):
        block_sum, decay = inputs
        return (carry * decay[:, None, None] + block_sum, carry)

    final, entering = lax.scan(
        advance, jnp.zeros((heads, width, state), jnp.float32), (block_sums, block_decay)
    )
    overall = jnp.exp(jnp.sum(log_decay[:, -1], axis=0))
    return (log_decay, scaled_values, entering, final, overall)


def block_outputs(reads, writes, log_decay, scaled_values, entering, start_state):
    count, block, heads = log_decay.shape
    state = reads.shape[2]
    read_blocks = reads.reshape(count, block, heads, state)
    write_blocks = writes.reshape(count, block, heads, state)
    starts = jnp.cumsum(log_decay[:, -1], axis=0) - log_decay[:, -1]
    entering_all = entering + jnp.exp(starts)[:, :, None, None] * start_state[None]
    forward_mask = jnp.tril(jnp.ones((block, block), bool))[None, :, :, None]
    spans = log_decay[:, :, None, :] - log_decay[:, None, :, :]
    weights = jnp.where(forward_mask, jnp.exp(jnp.where(forward_mask, spans, 0.0)), 0.0)
    intersection = jnp.einsum(
        "kqhn,kshn->kqsh", read_blocks, write_blocks, precision=lax.Precision.HIGHEST
    )
    within = jnp.einsum(
        "kqsh,kshp->kqhp", intersection * weights, scaled_values, precision=lax.Precision.HIGHEST
    )
    carried = (
        jnp.einsum("kqhn,khpn->kqhp", read_blocks, entering_all, precision=lax.Precision.HIGHEST)
        * jnp.exp(log_decay)[..., None]
    )
    return (within + carried).reshape(count * block, heads, -1)


def chain(earlier, later):
    return (earlier[0] * later[0], earlier[1] * later[0][:, None, None] + later[1])


def per_device(
    latent,
    context,
    cond,
    cond_ctx,
    mod_shift_w,
    mod_scale_w,
    mod_gate_w,
    norm_gain,
    proj_z,
    proj_x,
    proj_b,
    proj_c,
    proj_dt,
    conv_x,
    conv_b,
    conv_c,
    dt_bias,
    decay_log,
    head_gain,
    proj_out,
):
    heads = proj_x.shape[1] // HEAD_DIM
    state = proj_b.shape[1] // heads
    width_x = heads * HEAD_DIM
    width_b = heads * state
    act = jax.nn.silu(cond.astype(jnp.float32)).astype(jnp.bfloat16)
    act_ctx = jax.nn.silu(cond_ctx.astype(jnp.float32)).astype(jnp.bfloat16)
    stacked = jnp.stack([act, act_ctx])
    shift_part = jnp.dot(stacked, mod_shift_w, preferred_element_type=jnp.float32)
    scale_part = jnp.dot(stacked, mod_scale_w, preferred_element_type=jnp.float32)
    gate_part = jnp.dot(act[None], mod_gate_w, preferred_element_type=jnp.float32)
    shift_sum, scale_sum, gate_sum = lax.psum((shift_part, scale_part, gate_part), "sp")
    shifts, scales, gates = (
        lax.all_gather(shift_sum, "tp", axis=1, tiled=True),
        lax.all_gather(scale_sum, "tp", axis=1, tiled=True),
        lax.all_gather(gate_sum, "tp", axis=1, tiled=True),
    )
    normed_rows = modulated_norm(latent, norm_gain, shifts[0], scales[0])
    normed_ctx = modulated_norm(context, norm_gain, shifts[1], scales[1])
    dt_weight = lax.dynamic_slice_in_dim(proj_dt, lax.axis_index("tp") * (2 * heads), 2 * heads, 1)
    joined = jnp.concatenate(
        project(
            lax.all_gather(normed_rows, "tp", axis=0, tiled=True),
            (proj_x, proj_b, proj_c, proj_z, dt_weight),
        ),
        axis=1,
    )
    ctx_joined = lax.all_gather(
        jnp.concatenate(project(normed_ctx, (proj_x, proj_b, dt_weight)), axis=1),
        "sp",
        axis=0,
        tiled=True,
    )
    length = joined.shape[0]
    ctx_length = ctx_joined.shape[0]
    conv_end = width_x + 2 * width_b
    padded = extended(joined[:, :conv_end], (("sp", 0),), 1)
    convolved = centred_conv(padded, jnp.concatenate([conv_x, conv_b, conv_c], axis=1))
    values = convolved[:, :width_x].reshape(length, heads, HEAD_DIM)
    writes = convolved[:, width_x : width_x + width_b].reshape(length, heads, state)
    reads = convolved[:, width_x + width_b :].reshape(length, heads, state)
    z_in = joined[:, conv_end : conv_end + width_x]
    step_size = jax.nn.softplus(
        joined[:, conv_end + width_x :].astype(jnp.float32) + dt_bias
    ).reshape(length, heads, 2)
    decay_rate = jnp.exp(decay_log).reshape(heads, 2)
    ctx_conv = centred_conv(
        zero_pad(ctx_joined[:, : width_x + width_b]), jnp.concatenate([conv_x, conv_b], axis=1)
    )
    values_ctx = ctx_conv[:, :width_x].reshape(ctx_length, heads, HEAD_DIM)
    writes_ctx = ctx_conv[:, width_x:].reshape(ctx_length, heads, state)
    step_ctx = jax.nn.softplus(
        ctx_joined[:, width_x + width_b :].astype(jnp.float32) + dt_bias
    ).reshape(ctx_length, heads, 2)
    ctx_f = block_states(values_ctx, writes_ctx, step_ctx[:, :, 0], decay_rate[:, 0], BLOCK)[3]
    ctx_b = block_states(
        jnp.flip(values_ctx, 0),
        jnp.flip(writes_ctx, 0),
        jnp.flip(step_ctx[:, :, 1], 0),
        decay_rate[:, 1],
        BLOCK,
    )[3]
    log_f, scaled_f, enter_f, final_f, overall_f = block_states(
        values, writes, step_size[:, :, 0], decay_rate[:, 0], BLOCK
    )
    reads_back = jnp.flip(reads, 0)
    writes_back = jnp.flip(writes, 0)
    log_b, scaled_b, enter_b, final_b, overall_b = block_states(
        jnp.flip(values, 0), writes_back, jnp.flip(step_size[:, :, 1], 0), decay_rate[:, 1], BLOCK
    )
    identity = (jnp.ones((heads,), jnp.float32), jnp.zeros((heads, HEAD_DIM, state), jnp.float32))
    before = entering_2((overall_f, final_f), "sp", chain, identity, False)
    after = entering_2((overall_b, final_b), "sp", chain, identity, True)
    start_f = before[1] + before[0][:, None, None] * ctx_f
    start_b = after[1] + after[0][:, None, None] * ctx_b
    out_f = block_outputs(reads, writes, log_f, scaled_f, enter_f, start_f)
    out_b = block_outputs(reads_back, writes_back, log_b, scaled_b, enter_b, start_b)
    summed = out_f + jnp.flip(out_b, 0)
    gated = summed * jax.nn.silu(z_in.astype(jnp.float32)).reshape(length, heads, HEAD_DIM)
    gated = gated * lax.rsqrt(jnp.mean(gated * gated, axis=-1, keepdims=True) + EPS)
    gated = gated * head_gain.astype(jnp.float32).reshape(heads, HEAD_DIM)
    mixed_heads = gated.reshape(length, width_x).astype(jnp.bfloat16)
    update_cols = jnp.dot(
        lax.all_gather(mixed_heads, "tp", axis=1, tiled=True),
        proj_out,
        preferred_element_type=jnp.float32,
    )
    update_rows = lax.all_to_all(
        update_cols.astype(jnp.bfloat16), "tp", split_axis=0, concat_axis=1, tiled=True
    )
    update = lax.optimization_barrier(update_rows).astype(jnp.float32)
    return (latent.astype(jnp.float32) + gates[0] * update).astype(jnp.bfloat16)


MESH = pl.DeviceIdType.MESH
F32 = jnp.float32
BF16 = jnp.bfloat16


def silu(v):
    return v * (1.0 / (1.0 + jnp.exp(-v)))


def softplus(v):
    return jnp.maximum(v, 0.0) + jnp.log1p(jnp.exp(-jnp.abs(v)))


def dot_nt(a, b):
    return lax.dot_general(a, b, (((1,), (1,)), ((), ())), preferred_element_type=F32)


def dot_tn(a, b):
    return lax.dot_general(a, b, (((0,), (0,)), ((), ())), preferred_element_type=F32)


def dot_exact(a, b):
    return jnp.dot(a, b, preferred_element_type=F32, precision=lax.Precision.HIGHEST)


def iota(shape, dim):
    return lax.broadcasted_iota(jnp.int32, shape, dim)


def fused(
    sizes,
    latent,
    context,
    cond,
    cond_ctx,
    w_shift,
    w_scale,
    w_gate,
    gain,
    w_z,
    w_x,
    w_b,
    w_c,
    w_dt,
    taps_x,
    taps_b,
    taps_c,
    steps,
    head_gain,
    w_out,
    out,
    mod_w,
    w_all,
    dt_w,
    out_w,
    parts,
    sums,
    raw_rows,
    h,
    proj,
    proj_d,
    ctx_x,
    ctx_b,
    ctx_d,
    edge_first,
    edge_last,
    edge_before,
    edge_after,
    taps,
    conv,
    totals,
    states_out,
    states_in,
    ctx_states,
    heads_out,
    acc,
    upd,
    upd_in,
    load_sem,
    mod_send,
    mod_recv,
    sum_send,
    sum_recv,
    h_send,
    h_recv,
    m_send,
    m_recv,
    ctx_send,
    ctx_recv,
    edge_send,
    edge_recv,
    st_send,
    st_recv,
    tot_send,
    tot_recv,
    cs_send,
    cs_recv,
    up_send,
    up_recv,
):
    n_sp, n_tp, rows, ctx_rows, wx, wb, deep = sizes
    length = rows * n_tp
    ctx_len = ctx_rows * n_sp
    pairs = wx // 128
    chunk = wx
    sp = lax.axis_index("sp")
    tp = lax.axis_index("tp")
    core = tp % 2
    at_x = (tp // 2) % 2
    at_y = tp // 4

    def place(y, x, c):
        return y * 4 + x * 2 + c

    near_x = place(at_y, 1 - at_x, core)
    near_y = place(1 - at_y, at_x, core)
    mate = place(at_y, at_x, 1 - core)
    far = place(1 - at_y, 1 - at_x, core)
    mate_x = place(at_y, 1 - at_x, 1 - core)
    mate_y = place(1 - at_y, at_x, 1 - core)
    mate_far = place(1 - at_y, 1 - at_x, 1 - core)

    def sp_peer(d):
        return (sp + d) % n_sp

    def tp_peer(d):
        return (tp + d) % n_tp

    def remote(src, dst, send, recv, axis, to):
        return pltpu.make_async_remote_copy(
            src_ref=src,
            dst_ref=dst,
            send_sem=send,
            recv_sem=recv,
            device_id={axis: to},
            device_id_type=MESH,
        )

    loads = []
    mods = (w_shift, w_scale, w_gate)
    for k in range(3):
        loads.append(pltpu.make_async_copy(mods[k], mod_w.at[k], load_sem.at[k]))
    starts = (0, wx, wx + wb, wx + 2 * wb)
    for k, (src, lo, width) in enumerate(
        ((w_x, 0, wx), (w_b, wx, wb), (w_c, wx + wb, wb), (w_z, wx + 2 * wb, wx))
    ):
        loads.append(
            pltpu.make_async_copy(src, w_all.at[:, pl.ds(lo, width)], load_sem.at[3 + k])
        )
    loads.append(pltpu.make_async_copy(w_dt, dt_w, load_sem.at[7]))
    loads.append(pltpu.make_async_copy(w_out, out_w, load_sem.at[8]))
    for k in range(3):
        loads[k].start()

    barrier = pltpu.get_barrier_semaphore()
    for d in range(1, n_sp):
        pl.semaphore_signal(barrier, inc=1, device_id={"sp": sp_peer(d)}, device_id_type=MESH)
    for d in range(1, n_tp):
        pl.semaphore_signal(barrier, inc=1, device_id={"tp": tp_peer(d)}, device_id_type=MESH)

    half = rows // 2

    def h_at(slot, k):
        return raw_rows.at[pl.ds(pl.multiple_of(slot * rows + k * half, half), half)]

    def m_at(slot, k):
        return heads_out.at[slot, k]

    def exchange(at, send, recv, own=None):
        plan = {
            0: (tp, 0, near_x, near_x),
            1: (tp, 1, near_x, near_x),
            2: (tp, 0, near_y, near_y),
            3: (tp, 1, near_y, near_y),
            4: (tp, 0, mate, mate),
            5: (tp, 1, mate, mate),
            6: (near_x, 0, near_y, far),
            7: (near_y, 1, near_x, far),
            8: (near_x, 0, mate, mate_x),
            9: (near_x, 1, mate, mate_x),
            10: (near_y, 0, mate, mate_y),
            11: (near_y, 1, mate, mate_y),
            12: (far, 0, mate, mate_far),
            13: (far, 1, mate, mate_far),
        }
        live = {}

        def go(k):
            slot, part, to, _ = plan[k]
            src = own(part) if own is not None and k < 6 else at(slot, part)
            c = remote(src, at(slot, part), send.at[k], recv.at[k], "tp", to)
            c.start()
            live[k] = c

        def got(k):
            _, part, _, slot = plan[k]
            remote(at(slot, part), at(slot, part), send.at[k], recv.at[k], "tp", mate).wait_recv()
            return slot, part

        return go, got, live

    def own_half(k):
        return latent.at[pl.ds(k * half, half)]

    h_go, h_got, h_live = exchange(h_at, h_send, h_recv, own_half)
    pl.semaphore_wait(barrier, n_sp - 1 + n_tp - 1)
    for k in (0, 3, 1, 2, 4, 5):
        h_go(k)

    act = silu(cond[...].astype(F32).reshape(1, -1))
    act_ctx = silu(cond_ctx[...].astype(F32).reshape(1, -1))
    row = iota((16, act.shape[1]), 0)
    stacked = jnp.where(row == 0, act, jnp.where(row == 1, act_ctx, 0.0)).astype(BF16)
    for k in range(3):
        loads[k].wait()
        if k == 2:
            for other in (3, 4, 7, 5, 6, 8):
                loads[other].start()
        part = jnp.dot(stacked, mod_w[k], preferred_element_type=F32)
        parts[sp, :, k * chunk : (k + 1) * chunk] = part[0:2]

    sends = []
    for d in range(1, n_sp):
        c = remote(parts.at[sp], parts.at[sp], mod_send.at[d], mod_recv.at[d], "sp", sp_peer(d))
        c.start()
        sends.append(c)
    taps[0:3, 0:wx] = taps_x[...].astype(F32)
    taps[0:3, wx : wx + wb] = taps_b[...].astype(F32)
    taps[0:3, wx + wb : wx + 2 * wb] = taps_c[...].astype(F32)
    for d in range(1, n_sp):
        sends[d - 1].wait_recv()
    total = parts[0]
    for k in range(1, n_sp):
        total = total + parts[k]
    sums[tp] = total
    for d in range(1, n_tp):
        c = remote(sums.at[tp], sums.at[tp], sum_send.at[d], sum_recv.at[d], "tp", tp_peer(d))
        c.start()
        sends.append(c)
    h_got(0)
    h_go(6)
    h_go(8)
    h_got(3)
    h_go(7)
    h_go(11)
    h_got(1)
    h_go(9)
    h_got(2)
    h_go(10)
    for d in range(1, n_tp):
        sends[n_sp - 1 + d - 1].wait_recv()

    def normed(values, which, at):
        wide = values.astype(F32)
        inv = lax.rsqrt(jnp.mean(wide * wide, axis=-1, keepdims=True) + EPS)
        for j in range(n_tp):
            lo = j * chunk
            piece = wide[:, lo : lo + chunk] * inv * gain[lo : lo + chunk].astype(F32).reshape(1, -1)
            scale = sums[j, which : which + 1, chunk : 2 * chunk]
            shift = sums[j, which : which + 1, 0:chunk]
            h[pl.ds(at, rows), lo : lo + chunk] = (piece * (1.0 + scale) + shift).astype(BF16)

    def normed_block(slot):
        at = pl.multiple_of(slot * rows, rows)
        normed(raw_rows[pl.ds(at, rows)], 0, at)

    normed(latent[...], 0, pl.multiple_of(tp * rows, rows))
    for k in range(ctx_rows // rows):
        normed(context[k * rows : (k + 1) * rows], 1, length + k * rows)
    normed_block(near_x)
    normed_block(near_y)
    h_got(6)
    h_go(12)
    h_got(7)
    h_go(13)
    normed_block(far)
    for ks, slot in (((4, 5), mate), ((8, 9), mate_x), ((10, 11), mate_y), ((12, 13), mate_far)):
        for k in ks:
            h_got(k)
        normed_block(slot)

    tile = 256
    width = wx + 2 * wb
    early = wx + wb
    whole_rows = length + ctx_rows

    def project_tiles(count, lo, hi):
        def step(k, carry):
            cols = pl.ds(pl.multiple_of(k * tile, tile), tile)
            proj[0:count, cols] = jnp.dot(
                h[0:count], w_all[:, cols], preferred_element_type=F32
            ).astype(BF16)
            return carry

        lax.fori_loop(lo // tile, hi // tile, step, 0)

    edges = []

    def send_edges(lo, hi, at):
        edge_first[:, lo:hi] = proj[0:16, lo:hi].astype(F32)[0:1]
        edge_last[:, lo:hi] = proj[length - 16 : length, lo:hi].astype(F32)[15:16]
        cols = pl.ds(lo, hi - lo)
        for k, (src, dst, to) in enumerate(
            (
                (edge_last, edge_before, sp_peer(1)),
                (edge_first, edge_after, sp_peer(n_sp - 1)),
            )
        ):
            c = remote(
                src.at[:, cols],
                dst.at[:, cols],
                edge_send.at[at + k],
                edge_recv.at[at + k],
                "sp",
                to,
            )
            c.start()
            edges.append(c)

    loads[3].wait()
    loads[4].wait()
    loads[7].wait()
    project_tiles(whole_rows, 0, early)
    proj_d[...] = jnp.dot(h[...], dt_w[...], preferred_element_type=F32).astype(BF16)
    send_edges(0, early, 0)
    ctx_live = []
    for d in range(1, n_sp):
        to = sp_peer(d)
        x_cols = pl.ds(pl.multiple_of(to * 128, 128), 128)
        b_cols = pl.ds(pl.multiple_of(wx + to * 256, 128), 256)
        tail = pl.ds(length, ctx_rows)
        for k, (src, dst) in enumerate(
            (
                (proj.at[tail, x_cols], ctx_x.at[sp]),
                (proj.at[tail, b_cols], ctx_b.at[sp]),
                (proj_d.at[tail], ctx_d.at[sp]),
            )
        ):
            c = remote(src, dst, ctx_send.at[d, k], ctx_recv.at[d, k], "sp", to)
            c.start()
            ctx_live.append(c)
    ctx_x[sp] = proj[length : length + ctx_rows, pl.ds(pl.multiple_of(sp * 128, 128), 128)]
    ctx_b[sp] = proj[length : length + ctx_rows, pl.ds(pl.multiple_of(wx + sp * 256, 128), 256)]
    ctx_d[sp] = proj_d[length : length + ctx_rows]
    loads[5].wait()
    project_tiles(length, early, width)
    send_edges(early, width, 2)

    def conv_of(values, weights, before, after):
        count = values.shape[0]
        at = iota(values.shape, 0)
        prev = jnp.where(at == 0, before, pltpu.roll(values, 1, 0))
        post = jnp.where(at == count - 1, after, pltpu.roll(values, count - 1, 0))
        return silu(weights[0:1] * prev + weights[1:2] * values + weights[2:3] * post)

    local = 4 * pairs
    bias = steps[0:1, :]
    rate = jnp.exp(steps[1:2, :])
    diag = iota((local, 128), 0) == iota((local, 128), 1)
    bias_t = jnp.sum(jnp.where(diag, bias, 0.0), axis=1, keepdims=True)
    rate_t = jnp.sum(jnp.where(diag, rate, 0.0), axis=1, keepdims=True)
    sel_row = iota((128, 128), 0)
    pick = jnp.where(
        (iota((128, 128), 1) == sel_row + local * tp) & (sel_row < local), 1.0, 0.0
    ).astype(BF16)

    def decays(raw):
        count = raw.shape[0]
        step = softplus(dot_nt(raw, pick) + bias)
        rise = -(step * rate)
        r, c = iota((count, count), 0), iota((count, count), 1)
        lower = jnp.where(c <= r, 1.0, 0.0)
        upper = jnp.where(c >= r, 1.0, 0.0)
        fwd, bwd = dot_exact(lower, rise), dot_exact(upper, rise)
        even = iota(fwd.shape, 1) % 2 == 0
        total = fwd[count - 1 : count]
        mass = jnp.exp(total - jnp.where(even, fwd, bwd)) * step
        return fwd, bwd, total, mass, lower, upper

    lane = iota((1, 128), 1)

    def pair_states(values, b_one, b_two, f_one, f_two, r_one, r_two):
        first = lane < 64
        u_f = (values * jnp.where(first, f_one, f_two)).astype(BF16)
        u_b = (values * jnp.where(first, r_one, r_two)).astype(BF16)
        f1, f2 = dot_tn(u_f, b_one), dot_tn(u_f, b_two)
        r1, r2 = dot_tn(u_b, b_one), dot_tn(u_b, b_two)
        top = iota((128, 128), 0) < 64
        return jnp.where(top, f1, f2), jnp.where(top, r1, r2)

    raw = proj_d[0:length]
    fwd, bwd, total, mass, lower, upper = decays(raw)
    totals[sp] = total
    step_t = softplus(dot_nt(pick[0:local], raw) + bias_t)
    rise_t = -(step_t * rate_t)
    fwd_t, bwd_t = dot_exact(rise_t, upper), dot_exact(rise_t, lower)
    for c in edges[:2]:
        c.wait_recv()

    def conv_tile(k, carry):
        cols = pl.ds(pl.multiple_of(k * 128, 128), 128)
        before = jnp.where(sp > 0, edge_before[:, cols], 0.0)
        after = jnp.where(sp < n_sp - 1, edge_after[:, cols], 0.0)
        conv[:, cols] = conv_of(proj[0:length, cols].astype(F32), taps[:, cols], before, after)
        return carry

    lax.fori_loop(0, early // 128, conv_tile, 0)

    def b_of(head):
        return conv[:, wx + head * 128 : wx + head * 128 + 128].astype(BF16)

    def c_of(head):
        return conv[:, wx + wb + head * 128 : wx + wb + head * 128 + 128].astype(BF16)

    for p in range(pairs):
        base = 4 * p
        cols = [mass[:, base + k : base + k + 1] for k in range(4)]
        s_f, s_b = pair_states(
            conv[:, p * 128 : p * 128 + 128],
            b_of(2 * p),
            b_of(2 * p + 1),
            cols[0],
            cols[2],
            cols[1],
            cols[3],
        )
        states_out[0, p] = s_f.astype(BF16)
        states_out[1, p] = s_b.astype(BF16)
        states_in[sp, p] = jnp.zeros((128, 128), BF16)
    st_live = []
    for d in range(1, n_sp):
        which = (sp + d) // n_sp
        c = remote(
            states_out.at[which], states_in.at[sp], st_send.at[d], st_recv.at[d], "sp", sp_peer(d)
        )
        c.start()
        st_live.append(c)
        c = remote(totals.at[sp], totals.at[sp], tot_send.at[d], tot_recv.at[d], "sp", sp_peer(d))
        c.start()
        st_live.append(c)

    for c in ctx_live:
        c.wait_recv()
    raw_ctx = ctx_d[...].reshape(ctx_len, 128)
    mass_ctx = decays(raw_ctx)[3]
    x_taps = taps[:, pl.ds(pl.multiple_of(sp * 128, 128), 128)]
    b_taps = taps[:, pl.ds(pl.multiple_of(wx + sp * 256, 128), 256)]
    xs_c = conv_of(ctx_x[...].reshape(ctx_len, 128).astype(F32), x_taps, 0.0, 0.0)
    bs_c = conv_of(ctx_b[...].reshape(ctx_len, 256).astype(F32), b_taps, 0.0, 0.0).astype(BF16)

    def column(k):
        return jnp.sum(jnp.where(lane == 4 * sp + k, mass_ctx, 0.0), axis=1, keepdims=True)

    c_f, c_b = pair_states(
        xs_c, bs_c[:, :128], bs_c[:, 128:], column(0), column(2), column(1), column(3)
    )
    ctx_states[sp, 0] = c_f.astype(BF16)
    ctx_states[sp, 1] = c_b.astype(BF16)

    cs_live = []
    for d in range(1, n_sp):
        c = remote(
            ctx_states.at[sp], ctx_states.at[sp], cs_send.at[d], cs_recv.at[d], "sp", sp_peer(d)
        )
        c.start()
        cs_live.append(c)

    loads[6].wait()
    project_tiles(length, width, width + wx)
    for c in edges[2:]:
        c.wait_recv()
    lax.fori_loop(early // 128, width // 128, conv_tile, 0)

    r, c_i = iota((length, length), 0), iota((length, length), 1)
    below, same = c_i < r, c_i == r
    first = lane < 64
    inner = []
    for p in range(pairs):
        x_p = conv[:, p * 128 : p * 128 + 128].astype(BF16)
        found = []
        for head in (2 * p, 2 * p + 1):
            f, b = 2 * head, 2 * head + 1
            score = dot_nt(c_of(head), b_of(head))
            span = jnp.where(
                below,
                fwd[:, f : f + 1] - fwd_t[f : f + 1],
                bwd[:, b : b + 1] - bwd_t[b : b + 1],
            )
            step = jnp.where(below, step_t[f : f + 1], step_t[b : b + 1]) + jnp.where(
                same, step_t[f : f + 1], 0.0
            )
            weight = (score * (jnp.exp(span) * step)).astype(BF16)
            found.append(jnp.dot(weight, x_p, preferred_element_type=F32))
        acc[:, p * 128 : p * 128 + 128] = jnp.where(first, found[0], found[1])

    for c in cs_live + st_live:
        c.wait_recv()

    m_go, m_got, m_live = exchange(m_at, m_send, m_recv)
    top = iota((128, 128), 0) < 64
    for p in range(pairs):
        base = 4 * p
        carried = []
        for way in range(2):
            state = ctx_states[p, way].astype(F32)
            for k in range(n_sp):
                q = n_sp - 1 - k if way else k
                drop = jnp.exp(
                    jnp.where(
                        top,
                        totals[q, 0:1, base + way : base + way + 1],
                        totals[q, 0:1, base + 2 + way : base + 3 + way],
                    )
                )
                reached = q > sp if way else q < sp
                state = jnp.where(reached, state * drop + states_in[q, p].astype(F32), state)
            start = state.astype(BF16)
            one, two = dot_nt(c_of(2 * p), start), dot_nt(c_of(2 * p + 1), start)
            log = bwd if way else fwd
            fade = jnp.exp(
                jnp.where(
                    first,
                    log[:, base + way : base + way + 1],
                    log[:, base + 2 + way : base + 3 + way],
                )
            )
            carried.append(jnp.where(first, one, two) * fade)
        cols = slice(p * 128, p * 128 + 128)
        z_in = proj[0:length, width + p * 128 : width + p * 128 + 128].astype(F32)
        g = (acc[:, cols] + carried[0] + carried[1]) * silu(z_in)
        square = g * g
        mean_1 = jnp.sum(jnp.where(first, square, 0.0), axis=1, keepdims=True) / 64.0
        mean_2 = jnp.sum(jnp.where(first, 0.0, square), axis=1, keepdims=True) / 64.0
        inv = jnp.where(first, lax.rsqrt(mean_1 + EPS), lax.rsqrt(mean_2 + EPS))
        done = (g * inv * head_gain[cols].astype(F32).reshape(1, -1)).astype(BF16)
        per = pairs // 2
        heads_out[tp, p // per, :, (p % per) * 128 : (p % per) * 128 + 128] = done
        if p % per == per - 1:
            for k in ((0, 2, 4) if p // per == 0 else (3, 1, 5)):
                m_go(k)

    loads[8].wait()
    piece = wx // 2

    def gather_add(slot, k, fresh=False):
        at = pl.ds(pl.multiple_of(slot * wx + k * piece, piece), piece)
        new = jnp.dot(heads_out[slot, k], out_w[at, :], preferred_element_type=F32)
        acc[...] = new if fresh else acc[...] + new

    gather_add(tp, 0, True)
    gather_add(tp, 1)
    a = m_got(0)
    m_go(6)
    m_go(8)
    gather_add(*a)
    gather_add(*m_got(4))
    a = m_got(3)
    m_go(7)
    m_go(11)
    gather_add(*a)
    a = m_got(1)
    m_go(9)
    b = m_got(2)
    m_go(10)
    gather_add(*a)
    gather_add(*b)
    for k in (5, 8):
        gather_add(*m_got(k))
    a = m_got(6)
    m_go(12)
    b = m_got(7)
    m_go(13)
    gather_add(*a)
    gather_add(*b)
    for k in (11, 9, 10, 12, 13):
        gather_add(*m_got(k))

    upd[...] = acc[...].astype(BF16)
    up_live = []
    for d in range(1, n_tp):
        to = tp_peer(d)
        src = upd.at[pl.ds(pl.multiple_of(to * rows, rows), rows)]
        c = remote(src, upd_in.at[tp], up_send.at[d], up_recv.at[d], "tp", to)
        c.start()
        up_live.append(c)
    upd_in[tp] = upd[pl.ds(pl.multiple_of(tp * rows, rows), rows)]
    for c in up_live:
        c.wait_recv()
    for j in range(n_tp):
        cols = slice(j * chunk, (j + 1) * chunk)
        gate = sums[j, 0:1, 2 * chunk : 3 * chunk]
        out[:, cols] = (latent[:, cols].astype(F32) + gate * upd_in[j].astype(F32)).astype(BF16)
    for c in (
        sends
        + list(h_live.values())
        + ctx_live
        + cs_live
        + edges
        + st_live
        + list(m_live.values())
        + up_live
    ):
        c.wait_send()


def per_device_fused(
    n_sp,
    n_tp,
    latent,
    context,
    cond,
    cond_ctx,
    mod_shift_w,
    mod_scale_w,
    mod_gate_w,
    norm_gain,
    proj_z,
    proj_x,
    proj_b,
    proj_c,
    proj_dt,
    conv_x,
    conv_b,
    conv_c,
    dt_bias,
    decay_log,
    head_gain,
    proj_out,
):
    rows, deep = latent.shape
    ctx_rows = context.shape[0]
    wx, wb = proj_x.shape[1], proj_b.shape[1]
    length, pairs = rows * n_tp, wx // 128
    width = wx + 2 * wb
    steps = jnp.stack([dt_bias, decay_log])
    steps = jnp.pad(steps, ((0, 0), (0, 128 - steps.shape[1])))
    vmem = pl.BlockSpec(memory_space=pltpu.VMEM)
    hbm = pl.BlockSpec(memory_space=pl.ANY)
    dma = pltpu.SemaphoreType.DMA
    scratch = [
        pltpu.VMEM((3,) + mod_shift_w.shape, BF16),
        pltpu.VMEM((deep, width + wx), BF16),
        pltpu.VMEM(proj_dt.shape, BF16),
        pltpu.VMEM(proj_out.shape, BF16),
        pltpu.VMEM((n_sp, 2, 3 * wx), F32),
        pltpu.VMEM((n_tp, 2, 3 * wx), F32),
        pltpu.VMEM((length, deep), BF16),
        pltpu.VMEM((length + ctx_rows, deep), BF16),
        pltpu.VMEM((length + ctx_rows, width + wx), BF16),
        pltpu.VMEM((length + ctx_rows, 128), BF16),
        pltpu.VMEM((n_sp, ctx_rows, 128), BF16),
        pltpu.VMEM((n_sp, ctx_rows, 256), BF16),
        pltpu.VMEM((n_sp, ctx_rows, 128), BF16),
        pltpu.VMEM((1, width), F32),
        pltpu.VMEM((1, width), F32),
        pltpu.VMEM((1, width), F32),
        pltpu.VMEM((1, width), F32),
        pltpu.VMEM((8, width), F32),
        pltpu.VMEM((length, width), F32),
        pltpu.VMEM((n_sp, 1, 128), F32),
        pltpu.VMEM((2, pairs, 128, 128), BF16),
        pltpu.VMEM((n_sp, pairs, 128, 128), BF16),
        pltpu.VMEM((n_sp, 2, 128, 128), BF16),
        pltpu.VMEM((n_tp, 2, length, wx // 2), BF16),
        pltpu.VMEM((length, wx), F32),
        pltpu.VMEM((length, wx), BF16),
        pltpu.VMEM((n_tp, rows, wx), BF16),
        dma((9,)),
    ]
    for shape in (
        (n_sp,), (n_tp,), (14,), (14,), (n_sp, 3), (4,), (n_sp,), (n_sp,), (n_sp,), (n_tp,)
    ):
        scratch += [dma(shape), dma(shape)]
    return pl.pallas_call(
        functools.partial(fused, (n_sp, n_tp, rows, ctx_rows, wx, wb, deep)),
        out_shape=jax.ShapeDtypeStruct(latent.shape, BF16),
        in_specs=[vmem] * 4 + [hbm] * 3 + [vmem] + [hbm] * 5 + [vmem] * 5 + [hbm],
        out_specs=vmem,
        scratch_shapes=scratch,
        compiler_params=pltpu.CompilerParams(
            collective_id=0, has_side_effects=True, vmem_limit_bytes=62 * 1024 * 1024
        ),
    )(
        latent, context, cond, cond_ctx, mod_shift_w, mod_scale_w, mod_gate_w,
        norm_gain, proj_z, proj_x, proj_b, proj_c, proj_dt, conv_x, conv_b, conv_c,
        steps, head_gain, proj_out,
    )


def fits(mesh, latent, context, proj_x, proj_b, proj_dt):
    n_sp, n_tp = mesh.shape["sp"], mesh.shape["tp"]
    heads = proj_x.shape[1] // HEAD_DIM // n_tp
    rows, ctx_rows = latent.shape[0] // (n_sp * n_tp), context.shape[0] // n_sp
    return (
        n_tp == 8
        and heads == 2 * n_sp
        and heads % 4 == 0
        and proj_b.shape[1] == 2 * proj_x.shape[1]
        and proj_x.shape[1] == latent.shape[1]
        and proj_dt.shape[1] == 128
        and rows % 32 == 0
        and ctx_rows % rows == 0
    )


def solution(mesh):
    placed = (
        P(("sp", "tp"), None),
        P("sp", None),
        P("sp"),
        P("sp"),
        P("sp", "tp"),
        P("sp", "tp"),
        P("sp", "tp"),
        P(),
        P(None, "tp"),
        P(None, "tp"),
        P(None, "tp"),
        P(None, "tp"),
        P(),
        P(None, "tp"),
        P(None, "tp"),
        P(None, "tp"),
        P("tp"),
        P("tp"),
        P("tp"),
        P(None, "tp"),
    )
    def place(body):
        return jax.shard_map(
            body, mesh=mesh, in_specs=placed, out_specs=P(("sp", "tp"), None), check_vma=False
        )

    def step(*arrays):
        latent, context, proj_x, proj_b, proj_dt = (arrays[k] for k in (0, 1, 9, 10, 12))
        if fits(mesh, latent, context, proj_x, proj_b, proj_dt):
            return place(
                functools.partial(per_device_fused, mesh.shape["sp"], mesh.shape["tp"])
            )(*arrays)
        return place(per_device)(*arrays)

    return step
```

profile of v0, /device:TPU:0, one launch (start us, length us, event | category | flops | bytes accessed | tf_op | source)
XLA Modules:
  0.0 73.5 jit_solution(5851649418714739801)
XLA Ops:
  0.0 1.2 %select_maximum_fusion.steps = f32[2,128]{1,0:T(2,128)} fusion(f32[1,16]{1,0:T(1,128)} %bitcast.2, f32[1,16]{1,0:T(1,128)} %bitcast.3), kind=kLoop, calls=%fused_computation | loop fusion | flops 1024 | bytes 1152 | tf_op jit(solution)/shard_map/stack | solution.py:884
  1.2 70.6 %shard_map.190 = bf16[32,4096]{1,0:T(8,128)(2,1)} custom-call(bf16[32,4096]{1,0:T(8,128)(2,1)} %latent.1, bf16[64,4096]{1,0:T(8,128)(2,1)} %context.1, bf16[1024]{0:T(1024)(128)(2,1)} %cond.1, bf16[1024]{0:T(1024)(128)(2,1)} %cond_ctx.1, bf16[1024,512]{1,0:T(8,128)(2,1)} %w_shift.1, bf16[1024,512]{1,0:T(8,128)(2,1)} %w_scale.1, bf16[1024,512]{1,0:T(8,128)(2,1)} %w_gate.1, ...), custom_call_target="tpu_custom_call" | custom-call | tf_op jit(solution)/shard_map/pallas_call | solution.py:923
  71.8 1.7 %copy.22 = bf16[32,4096]{1,0:T(8,128)(2,1)} copy(bf16[32,4096]{1,0:T(8,128)(2,1)} %shard_map.190) | data formatting | bytes 524288
where the time goes:
time: 73.7 us; the launch traced here: 73.5 us
  Pallas kernels  70.6 us (96%)
  local copies, waits for them, and re-layouts  1.67 us (2%)
  other arithmetic  1.24 us (2%)
    pallas_call x1, Pallas kernels, per_device_fused(): pl.pallas_call(functools.partial(fused, (n_sp, n_tp, rows, ctx_rows, wx,...  70.6 us
    unnamed x1, local copies, waits for them, and re-layouts  1.67 us

commit v1 on v0

--- a/solution.py
+++ b/solution.py
@@ -278,26 +278,38 @@
 
 def fused(
     sizes,
-    latent,
-    context,
-    cond,
-    cond_ctx,
+    latent_hbm,
+    context_hbm,
+    cond_hbm,
+    cond_ctx_hbm,
     w_shift,
     w_scale,
     w_gate,
-    gain,
+    gain_hbm,
     w_z,
     w_x,
     w_b,
     w_c,
     w_dt,
+    taps_x_hbm,
+    taps_b_hbm,
+    taps_c_hbm,
+    bias_hbm,
+    decay_hbm,
+    head_gain_hbm,
+    w_out,
+    out,
+    context,
+    cond,
+    cond_ctx,
+    gain,
     taps_x,
     taps_b,
     taps_c,
+    bias_own,
+    decay_own,
+    head_gain,
     steps,
-    head_gain,
-    w_out,
-    out,
     mod_w,
     w_all,
     dt_w,
@@ -326,6 +338,7 @@
     upd,
     upd_in,
     load_sem,
+    small_sem,
     mod_send,
     mod_recv,
     sum_send,
@@ -398,14 +411,37 @@
         )
     loads.append(pltpu.make_async_copy(w_dt, dt_w, load_sem.at[7]))
     loads.append(pltpu.make_async_copy(w_out, out_w, load_sem.at[8]))
-    for k in range(3):
-        loads[k].start()
+    own_rows = pl.ds(pl.multiple_of(tp * rows, rows), rows)
+    small = [
+        pltpu.make_async_copy(src, dst, small_sem.at[k])
+        for k, (src, dst) in enumerate(
+            (
+                (latent_hbm, raw_rows.at[own_rows]),
+                (cond_hbm, cond),
+                (cond_ctx_hbm, cond_ctx),
+                (context_hbm, context),
+                (gain_hbm, gain),
+                (taps_x_hbm, taps_x),
+                (taps_b_hbm, taps_b),
+                (taps_c_hbm, taps_c),
+                (bias_hbm, bias_own),
+                (decay_hbm, decay_own),
+                (head_gain_hbm, head_gain),
+            )
+        )
+    ]
 
     barrier = pltpu.get_barrier_semaphore()
     for d in range(1, n_sp):
         pl.semaphore_signal(barrier, inc=1, device_id={"sp": sp_peer(d)}, device_id_type=MESH)
     for d in range(1, n_tp):
         pl.semaphore_signal(barrier, inc=1, device_id={"tp": tp_peer(d)}, device_id_type=MESH)
+    for c in small[:3]:
+        c.start()
+    for k in range(3):
+        loads[k].start()
+    for c in small[3:]:
+        c.start()
 
     half = rows // 2
 
@@ -415,7 +451,7 @@
     def m_at(slot, k):
         return heads_out.at[slot, k]
 
-    def exchange(at, send, recv, own=None):
+    def exchange(at, send, recv):
         plan = {
             0: (tp, 0, near_x, near_x),
             1: (tp, 1, near_x, near_x),
@@ -436,8 +472,7 @@
 
         def go(k):
             slot, part, to, _ = plan[k]
-            src = own(part) if own is not None and k < 6 else at(slot, part)
-            c = remote(src, at(slot, part), send.at[k], recv.at[k], "tp", to)
+            c = remote(at(slot, part), at(slot, part), send.at[k], recv.at[k], "tp", to)
             c.start()
             live[k] = c
 
@@ -448,14 +483,14 @@
 
         return go, got, live
 
-    def own_half(k):
-        return latent.at[pl.ds(k * half, half)]
-
-    h_go, h_got, h_live = exchange(h_at, h_send, h_recv, own_half)
+    h_go, h_got, h_live = exchange(h_at, h_send, h_recv)
+    small[0].wait()
     pl.semaphore_wait(barrier, n_sp - 1 + n_tp - 1)
     for k in (0, 3, 1, 2, 4, 5):
         h_go(k)
 
+    for c in small[1:3]:
+        c.wait()
     act = silu(cond[...].astype(F32).reshape(1, -1))
     act_ctx = silu(cond_ctx[...].astype(F32).reshape(1, -1))
     row = iota((16, act.shape[1]), 0)
@@ -473,6 +508,12 @@
         c = remote(parts.at[sp], parts.at[sp], mod_send.at[d], mod_recv.at[d], "sp", sp_peer(d))
         c.start()
         sends.append(c)
+    for c in small[3:]:
+        c.wait()
+    local = 4 * pairs
+    steps[...] = jnp.zeros_like(steps)
+    steps[0:1, 0:local] = bias_own[...]
+    steps[1:2, 0:local] = decay_own[...]
     taps[0:3, 0:wx] = taps_x[...].astype(F32)
     taps[0:3, wx : wx + wb] = taps_b[...].astype(F32)
     taps[0:3, wx + wb : wx + 2 * wb] = taps_c[...].astype(F32)
@@ -513,7 +554,7 @@
         at = pl.multiple_of(slot * rows, rows)
         normed(raw_rows[pl.ds(at, rows)], 0, at)
 
-    normed(latent[...], 0, pl.multiple_of(tp * rows, rows))
+    normed_block(tp)
     for k in range(ctx_rows // rows):
         normed(context[k * rows : (k + 1) * rows], 1, length + k * rows)
     normed_block(near_x)
@@ -602,7 +643,6 @@
         post = jnp.where(at == count - 1, after, pltpu.roll(values, count - 1, 0))
         return silu(weights[0:1] * prev + weights[1:2] * values + weights[2:3] * post)
 
-    local = 4 * pairs
     bias = steps[0:1, :]
     rate = jnp.exp(steps[1:2, :])
     diag = iota((local, 128), 0) == iota((local, 128), 1)
@@ -838,7 +878,7 @@
     for j in range(n_tp):
         cols = slice(j * chunk, (j + 1) * chunk)
         gate = sums[j, 0:1, 2 * chunk : 3 * chunk]
-        out[:, cols] = (latent[:, cols].astype(F32) + gate * upd_in[j].astype(F32)).astype(BF16)
+        out[:, cols] = (raw_rows[own_rows, cols].astype(F32) + gate * upd_in[j].astype(F32)).astype(BF16)
     for c in (
         sends
         + list(h_live.values())
@@ -881,12 +921,15 @@
     wx, wb = proj_x.shape[1], proj_b.shape[1]
     length, pairs = rows * n_tp, wx // 128
     width = wx + 2 * wb
-    steps = jnp.stack([dt_bias, decay_log])
-    steps = jnp.pad(steps, ((0, 0), (0, 128 - steps.shape[1])))
+    bias, decay = dt_bias[None], decay_log[None]
     vmem = pl.BlockSpec(memory_space=pltpu.VMEM)
-    hbm = pl.BlockSpec(memory_space=pl.ANY)
+    hbm = pl.BlockSpec(memory_space=pltpu.HBM)
     dma = pltpu.SemaphoreType.DMA
-    scratch = [
+    small = (
+        context, cond, cond_ctx, norm_gain, conv_x, conv_b, conv_c, bias, decay, head_gain,
+    )
+    scratch = [pltpu.VMEM(a.shape, a.dtype) for a in small] + [
+        pltpu.VMEM((8, 128), F32),
         pltpu.VMEM((3,) + mod_shift_w.shape, BF16),
         pltpu.VMEM((deep, width + wx), BF16),
         pltpu.VMEM(proj_dt.shape, BF16),
@@ -915,6 +958,7 @@
         pltpu.VMEM((length, wx), BF16),
         pltpu.VMEM((n_tp, rows, wx), BF16),
         dma((9,)),
+        dma((11,)),
     ]
     for shape in (
         (n_sp,), (n_tp,), (14,), (14,), (n_sp, 3), (4,), (n_sp,), (n_sp,), (n_sp,), (n_tp,)
@@ -922,17 +966,17 @@
         scratch += [dma(shape), dma(shape)]
     return pl.pallas_call(
         functools.partial(fused, (n_sp, n_tp, rows, ctx_rows, wx, wb, deep)),
-        out_shape=jax.ShapeDtypeStruct(latent.shape, BF16),
-        in_specs=[vmem] * 4 + [hbm] * 3 + [vmem] + [hbm] * 5 + [vmem] * 5 + [hbm],
+        out_shape=pltpu.VMEM(latent.shape, BF16),
+        in_specs=[hbm] * 20,
         out_specs=vmem,
         scratch_shapes=scratch,
         compiler_params=pltpu.CompilerParams(
-            collective_id=0, has_side_effects=True, vmem_limit_bytes=62 * 1024 * 1024
+            collective_id=0, has_side_effects=True, vmem_limit_bytes=60 * 1024 * 1024
         ),
     )(
         latent, context, cond, cond_ctx, mod_shift_w, mod_scale_w, mod_gate_w,
         norm_gain, proj_z, proj_x, proj_b, proj_c, proj_dt, conv_x, conv_b, conv_c,
-        steps, head_gain, proj_out,
+        bias, decay, head_gain, proj_out,
     )
 
 

time: 73.7 us -> 69.5 us (0.943)
  Pallas kernels: 70.6 us -> 68.7 us
  other arithmetic: 1.24 us -> 0 us
  local copies, waits for them, and re-layouts: 1.67 us -> 0.71 us
    pallas_call x1, Pallas kernels: 70.6 us -> 68.7 us  [per_device_fused(): pl.pallas_call(functools.partial(fused, (n_sp, n_tp, rows, ctx_rows, wx,...]
    another operation x1 -> x0, other arithmetic: 1.24 us -> none  [per_device_fused(): steps = jnp.stack([dt_bias, decay_log])]
    unnamed x1, local copies, waits for them, and re-layouts: 1.67 us -> 0.71 us
where the time goes in v1:
time: 69.5 us; the launch traced here: 69.4 us
  Pallas kernels  68.7 us (99%)
  local copies, waits for them, and re-layouts  0.71 us (1%)
    pallas_call x1, Pallas kernels, per_device_fused(): pl.pallas_call(functools.partial(fused, (n_sp, n_tp, rows, ctx_rows, wx,...  68.7 us

profile of v1, /device:TPU:0, one launch (start us, length us, event | category | flops | bytes accessed | tf_op | source)
XLA Modules:
  0.0 69.4 jit_solution(12240404688129039985)
XLA Ops:
  0.0 68.7 %shard_map.190 = bf16[32,4096]{1,0:T(8,128)(2,1)S(1)} custom-call(bf16[32,4096]{1,0:T(8,128)(2,1)} %latent_hbm.1, bf16[64,4096]{1,0:T(8,128)(2,1)} %context_hbm.1, bf16[1024]{0:T(1024)(128)(2,1)} %cond_hbm.1, bf16[1024]{0:T(1024)(128)(2,1)} %cond_ctx_hbm.1, bf16[1024,512]{1,0:T(8,128)(2,1)} %w_shift.1, bf16[1024,512]{1,0:T(8,128)(2,1)} %w_scale.1, ...), custom_call_target="tpu_custom_call" | custom-call | tf_op jit(solution)/shard_map/pallas_call | solution.py:967
  68.7 0.7 %copy.22 = bf16[32,4096]{1,0:T(8,128)(2,1)} copy(bf16[32,4096]{1,0:T(8,128)(2,1)S(1)} %shard_map.190) | data formatting | bytes 524288
